TPU v7x, 512 devices: a whole 4x4x16 slice. The times are simulated.
512 devices in a mesh: sp: 64 (over z, y), tp: 8 (over x, core).
Axes of the slice: x: 4, y: 4, z: 16, core: 2. Of those that a mesh axis runs over, the one named last changes fastest.
Arguments:
- latent: bfloat16 [49152, 2048], P(('sp', 'tp')), may hold values from -6 to 6
- condition: float32 [2048], P('sp'), may hold values from -6 to 6
- context_condition: float32 [2048], P('sp'), may hold values from -6 to 6
- context: bfloat16 [1024, 2048], P('sp'), may hold values from -6 to 6
- norm_gain: float32 [2048], replicated, may hold values from 0.1 to 1.9
- shift_weight: bfloat16 [2048, 2048], P('sp', 'tp'), may hold values from -0.375 to 0.375
- scale_weight: bfloat16 [2048, 2048], P('sp', 'tp'), may hold values from -0.375 to 0.375
- gate_weight: bfloat16 [2048, 2048], P('sp', 'tp'), may hold values from -0.375 to 0.375
- query_weight: bfloat16 [2048, 2048], P(None, 'tp'), may hold values from -2 to 2
- key_matrix: bfloat16 [2048, 1024], P(None, 'tp'), may hold values from -2 to 2
- value_matrix: bfloat16 [2048, 1024], P(None, 'tp'), may hold values from -0.125 to 0.125
- sink_logit_head: float32 [16], P('tp'), may hold values from 6 to 10
- out_weight: bfloat16 [2048, 2048], P('tp'), may hold values from -0.125 to 0.125
Outputs:
- updated: bfloat16 [49152, 2048], P(('sp', 'tp'))
All inputs are finite; a program needn't handle non-finite values.
Results may differ from a plain program's by a relative error of at most 0.012.
The roundings to bfloat16 on the way count: a program that leaves them out, or rounds other values in their place, can miss the bound.
Values may be sent and summed in bfloat16 or wider, within the bound.
A program may use at most 64 MiB of HBM per device.

v0:
```python
import functools
import jax
import jax.numpy as jnp
from jax import lax
from jax.sharding import Mesh
from jax.sharding import PartitionSpec as P

QUERY_HEADS = 16
KEY_VALUE_HEADS = 8
HEAD_DIM = 128
WINDOW_REACH = 128
GRID_W = 64
SP = ("sp_0", "sp_1")
SP_TP = ("sp_0", "sp_1", "tp")
NORM_EPS = 1e-05
MASKED_SCORE = -1e30


def one_axis_at_a_time(x, axes):
    return functools.reduce(lax.psum, axes, x)


def side_by_side(arrays, axis, dim, along):
    both = jnp.concatenate(arrays, axis=along)
    out, at, outs = (lax.all_gather(both, axis, axis=dim, tiled=True), 0, [])
    for a in arrays:
        outs.append(lax.slice_in_dim(out, at, at + a.shape[along], axis=along))
        at += a.shape[along]
    return tuple(outs)


def padded_2(block, sides, width):
    for axis, dim in sides:
        count = lax.axis_size(axis)
        forward = [(i, i + 1) for i in range(count - 1)]
        backward = [(target, source) for source, target in forward]
        low = lax.ppermute(
            lax.slice_in_dim(block, block.shape[dim] - width, None, axis=dim), axis, forward
        )
        high = lax.ppermute(lax.slice_in_dim(block, 0, width, axis=dim), axis, backward)
        block = jnp.concatenate([low, block, high], axis=dim)
    return block


def sent_to_all(x, axis):
    peers = lax.axis_size(axis)
    return lax.all_to_all(jnp.broadcast_to(x[None], (peers, *x.shape)), axis, 0, 0, tiled=True)


def laid_out(blocks, dim):
    blocks = jnp.moveaxis(blocks, 0, dim)
    shape = blocks.shape
    return blocks.reshape(*shape[:dim], shape[dim] * shape[dim + 1], *shape[dim + 2 :])


def gathered_copies(x, axis, dim):
    blocks = sent_to_all(x, axis)
    return laid_out(blocks, dim)


def in_blocks(x, dim, peers):
    before, after = (x.shape[:dim], x.shape[dim + 1 :])
    return jnp.moveaxis(x.reshape(*before, peers, -1, *after), dim, 0)


def summed_on_arrival(x, axis, dim):
    peers = lax.axis_size(axis)
    blocks = lax.all_to_all(in_blocks(x, dim, peers), axis, 0, 0, tiled=True)
    return jnp.sum(blocks.astype(jnp.float32), axis=0)


def rotate(vectors, position):
    quarter = HEAD_DIM // 4
    grid_row = (position // GRID_W).astype(jnp.float32)
    grid_col = (position % GRID_W).astype(jnp.float32)
    inv_freq = 10000.0 ** (-jnp.arange(0, HEAD_DIM // 2, 2, dtype=jnp.float32) / (HEAD_DIM // 2))
    angles = jnp.concatenate([grid_row[:, None] * inv_freq, grid_col[:, None] * inv_freq], axis=-1)
    cosine_table = jnp.cos(angles).reshape(-1, 1, 2, quarter)
    sine_table = jnp.sin(angles).reshape(-1, 1, 2, quarter)
    pieces = vectors.reshape(vectors.shape[0], vectors.shape[1], 2, 2, quarter)
    first_half = pieces[..., 0, :]
    second_half = pieces[..., 1, :]
    turned = jnp.stack(
        [
            first_half * cosine_table - second_half * sine_table,
            first_half * sine_table + second_half * cosine_table,
        ],
        axis=-2,
    )
    return turned.reshape(vectors.shape)


def modulated_norm(rows_in, norm_gain, shift, scale):
    floats = rows_in.astype(jnp.float32)
    normed = (
        floats * lax.rsqrt(jnp.mean(floats * floats, axis=-1, keepdims=True) + NORM_EPS) * norm_gain
    )
    return (normed * (1.0 + scale) + shift).astype(jnp.bfloat16)


def shards(
    latent,
    condition,
    context_condition,
    context,
    norm_gain,
    shift_weight,
    scale_weight,
    gate_weight,
    query_weight,
    key_matrix,
    value_matrix,
    sink_logit_head,
    out_weight,
):
    tp_count = lax.axis_size("tp")
    group_rows = latent.shape[0] * tp_count
    offset = lax.axis_index(SP) * group_rows
    total_rows = group_rows * lax.axis_size(SP)
    active = jax.nn.silu(jnp.stack([condition, context_condition])).astype(jnp.bfloat16)
    shift_part = jnp.dot(active, shift_weight, preferred_element_type=jnp.float32)
    scale_part = jnp.dot(active, scale_weight, preferred_element_type=jnp.float32)
    gate_part = jnp.dot(active[:1], gate_weight, preferred_element_type=jnp.float32)
    shift_sum, scale_sum, gate_sum = (
        one_axis_at_a_time(shift_part, SP),
        one_axis_at_a_time(scale_part, SP),
        one_axis_at_a_time(gate_part, SP),
    )
    shift_all, scale_all, gate_all = side_by_side((shift_sum, scale_sum, gate_sum), "tp", 1, 0)
    hidden_state = modulated_norm(latent, norm_gain, shift_all[0], scale_all[0])
    query_width = query_weight.shape[1]
    pair_width = key_matrix.shape[1]
    block_rows = lax.all_gather(hidden_state, "tp", axis=0, tiled=True)
    row_count = block_rows.shape[0]
    position = offset + jnp.arange(row_count, dtype=jnp.int32)
    query_row_block = jnp.dot(block_rows, query_weight, preferred_element_type=jnp.float32)
    query_row_block = rotate(query_row_block.reshape(row_count, -1, HEAD_DIM), position)
    key_rows = jnp.dot(block_rows, key_matrix, preferred_element_type=jnp.float32)
    key_rows = rotate(key_rows.reshape(row_count, -1, HEAD_DIM), position)
    value_rows = jnp.dot(block_rows, value_matrix, preferred_element_type=jnp.float32)
    projected = jnp.concatenate(
        [
            query_row_block.reshape(row_count, query_width),
            key_rows.reshape(row_count, pair_width),
            value_rows,
        ],
        axis=1,
    ).astype(jnp.bfloat16)
    padded = padded_2(projected[:, query_width:], ((SP, 0),), WINDOW_REACH)
    ctx_hidden = modulated_norm(context, norm_gain, shift_all[1], scale_all[1])
    ctx_pairs = gathered_copies(
        jnp.concatenate(
            [
                jnp.dot(ctx_hidden, key_matrix, preferred_element_type=jnp.float32),
                jnp.dot(ctx_hidden, value_matrix, preferred_element_type=jnp.float32),
            ],
            axis=1,
        ).astype(jnp.bfloat16),
        SP,
        0,
    )
    blocks = group_rows // WINDOW_REACH
    kv_local = pair_width // HEAD_DIM
    queries_per_group = QUERY_HEADS // KEY_VALUE_HEADS
    query_blocks = projected[:, :query_width].reshape(
        blocks, WINDOW_REACH, kv_local, queries_per_group, HEAD_DIM
    )
    key_pad = padded[:, :pair_width].reshape(blocks + 2, WINDOW_REACH, kv_local, HEAD_DIM)
    value_pad = padded[:, pair_width:].reshape(blocks + 2, WINDOW_REACH, kv_local, HEAD_DIM)
    band_keys = jnp.concatenate([key_pad[:-2], key_pad[1:-1], key_pad[2:]], axis=1)
    band_values = jnp.concatenate([value_pad[:-2], value_pad[1:-1], value_pad[2:]], axis=1)
    context_key_rows = ctx_pairs[:, :pair_width].reshape(-1, kv_local, HEAD_DIM)
    context_value_rows = ctx_pairs[:, pair_width:].reshape(-1, kv_local, HEAD_DIM)
    factor = HEAD_DIM ** (-0.5)
    band_scores = (
        jnp.einsum("nqhgd,nkhd->nhgqk", query_blocks, band_keys, preferred_element_type=jnp.float32)
        * factor
    )
    block_ids = jnp.arange(blocks, dtype=jnp.int32)[:, None, None]
    query_pos = (
        offset + block_ids * WINDOW_REACH + jnp.arange(WINDOW_REACH, dtype=jnp.int32)[None, :, None]
    )
    key_pos = (
        offset
        + (block_ids - 1) * WINDOW_REACH
        + jnp.arange(3 * WINDOW_REACH, dtype=jnp.int32)[None, None, :]
    )
    allowed = (
        (jnp.abs(key_pos - query_pos) <= WINDOW_REACH) & (key_pos >= 0) & (key_pos < total_rows)
    )
    band_scores = jnp.where(allowed[:, None, None], band_scores, MASKED_SCORE)
    ctx_scores = (
        jnp.einsum(
            "nqhgd,chd->nhgqc", query_blocks, context_key_rows, preferred_element_type=jnp.float32
        )
        * factor
    )
    sink_logit_rows = sink_logit_head.reshape(1, kv_local, queries_per_group, 1, 1)
    maxima = jnp.maximum(
        jnp.maximum(
            jnp.max(band_scores, axis=-1, keepdims=True),
            jnp.max(ctx_scores, axis=-1, keepdims=True),
        ),
        sink_logit_rows,
    )
    band_exp = jnp.exp(band_scores - maxima)
    ctx_exp = jnp.exp(ctx_scores - maxima)
    denominator = (
        jnp.sum(band_exp, axis=-1, keepdims=True)
        + jnp.sum(ctx_exp, axis=-1, keepdims=True)
        + jnp.exp(sink_logit_rows - maxima)
    )
    band_weights = (band_exp / denominator).astype(jnp.bfloat16)
    ctx_weights = (ctx_exp / denominator).astype(jnp.bfloat16)
    attended = jnp.einsum(
        "nhgqk,nkhd->nqhgd", band_weights, band_values, preferred_element_type=jnp.float32
    ) + jnp.einsum(
        "nhgqc,chd->nqhgd", ctx_weights, context_value_rows, preferred_element_type=jnp.float32
    )
    attended = attended.astype(jnp.bfloat16).reshape(group_rows, query_width)
    mixed_sum = summed_on_arrival(
        jnp.dot(attended, out_weight, preferred_element_type=jnp.float32).astype(jnp.bfloat16),
        "tp",
        0,
    )
    return (latent.astype(jnp.float32) + gate_all[0] * mixed_sum).astype(jnp.bfloat16)


def solution(mesh):
    torus = Mesh(mesh.devices.reshape(16, 4, mesh.shape["tp"]), ("sp_0", "sp_1", "tp"))
    return jax.shard_map(
        shards,
        mesh=torus,
        in_specs=(
            P(SP_TP, None),
            P(SP),
            P(SP),
            P(SP, None),
            P(),
            P(SP, "tp"),
            P(SP, "tp"),
            P(SP, "tp"),
            P(None, "tp"),
            P(None, "tp"),
            P(None, "tp"),
            P("tp"),
            P("tp", None),
        ),
        out_specs=P(SP_TP, None),
        check_vma=False,
    )
```

profile of v0, /device:TPU:128, one launch (start us, length us, event | category | flops | bytes accessed | tf_op | source)
XLA Modules:
  0.0 187.9 jit_solution(3284651303342493575)
XLA Ops:
  6.6 1.3 fusion.20
  11.1 30.9 %all-reduce = (f32[1,256]{1,0:T(1,128)S(1)}, f32[2,256]{1,0:T(2,128)S(1)}, f32[2,256]{1,0:T(2,128)S(1)}) all-reduce(f32[1,256]{1,0:T(1,128)S(1)} %fusion.59, f32[2,256]{1,0:T(2,128)S(1)} %fusion.71, f32[2,256]{1,0:T(2,128)S(1)} %fusion.70), channel_id=1, replica_groups=mesh['sp_0'=16,'sp_1'=4,'tp'=8] {'sp_0'}, use_global_device_ids=true, to_apply=%region_4.5 | all-reduce | flops 1280 | bytes 10240 | tf_op jit(solution)/shard_map/psum | solution.py:20
  42.0 10.8 %all-reduce.1 = (f32[1,256]{1,0:T(1,128)S(1)}, f32[2,256]{1,0:T(2,128)S(1)}, f32[2,256]{1,0:T(2,128)S(1)}) all-reduce(f32[1,256]{1,0:T(1,128)S(1)} %get-tuple-element.5, f32[2,256]{1,0:T(2,128)S(1)} %get-tuple-element.6, f32[2,256]{1,0:T(2,128)S(1)} %get-tuple-element.7), channel_id=1, replica_groups=mesh['sp_0'=16,'sp_1'=4,'tp'=8] {'sp_1'}, use_global_device_ids=true, to_apply=%region_5.6 | all-reduce | flops 1280 | bytes 10240 | tf_op jit(solution)/shard_map/psum | solution.py:20
  52.9 13.1 %all_gather.6 = f32[5,2048]{1,0:T(8,128)S(1)} all-gather(f32[5,256]{1,0:T(8,128)S(1)} %pad_maximum_fusion.12), channel_id=1, replica_groups=mesh['sp_0'=16,'sp_1'=4,'tp'=8] {'tp'}, dimensions={1}, use_global_device_ids=true | all-gather | bytes 46080 | tf_op jit(solution)/shard_map/all_gather | solution.py:25
  66.0 2.0 %fusion.24 = bf16[96,2048]{1,0:T(8,128)(2,1)} fusion(bf16[96,2048]{1,0:T(8,128)(2,1)} %param.13, f32[2048]{0:T(1024)S(1)} %bitcast.156, f32[2048]{0:T(1024)S(1)} %bitcast.157, f32[2048]{0:T(1024)} %param.17, f32[96]{0:T(128)S(1)} %add_rsqrt_fusion.1), kind=kLoop, calls=%fused_computation.34 | loop fusion | flops 1179648 | bytes 811392 | tf_op jit(solution)/shard_map/convert_element_type | solution.py:98
  68.0 1.0 fusion.42
  69.0 1.3 convolution_convert_fusion.2
  70.6 0.8 broadcast_in_dim.12
  71.5 12.3 %all-to-all-start = ((bf16[64,16,256]{2,1,0:T(8,128)(2,1)}), bf16[64,16,256]{2,1,0:T(8,128)(2,1)S(1)}, u32[]{:S(2)}, u32[]{:S(2)}) async-start(bf16[64,16,256]{2,1,0:T(8,128)(2,1)} %broadcast_in_dim.12), calls=%async_computation | async-start | bytes 1048576 | tf_op jit(solution)/shard_map/all_to_all | solution.py:47
  84.8 1.4 fusion.18
  86.2 14.9 %all-gather.2.cloned.1.call-done = bf16[768,2048]{1,0:T(8,128)(2,1)} async-done(((bf16[96,2048]{1,0:T(8,128)(2,1)}), bf16[768,2048]{1,0:T(8,128)(2,1)}) %all-gather.2.cloned.1.call-update) | async-done | bytes 3145744 | tf_op jit(solution)/shard_map/all_gather | solution.py:133
  101.2 3.0 %fusion.72 = f32[768,128]{0,1:T(8,128)S(1)} fusion(bf16[768,2048]{1,0:T(8,128)(2,1)} %all-gather.2.cloned.1.call-done, bf16[2048,128]{1,0:T(8,128)(2,1)S(1)} %copy-done.3), kind=kOutput, calls=%fused_computation.126 | convolution fusion | flops 402653184 | bytes 4063232 | tf_op jit(solution)/shard_map/dot_general | solution.py:138
  105.2 3.0 %convolution_convert_fusion.1 = bf16[768,128]{1,0:T(8,128)(2,1)S(1)} fusion(bf16[768,2048]{1,0:T(8,128)(2,1)} %all-gather.2.cloned.1.call-done, bf16[2048,128]{1,0:T(8,128)(2,1)S(1)} %copy-done.5), kind=kOutput, calls=%fused_computation.27 | convolution fusion | flops 402751488 | bytes 3866624 | tf_op jit(solution)/shard_map/dot_general | solution.py:140
  108.9 3.4 %collective-permute-start = (bf16[128,256]{1,0:T(8,128)(2,1)}, bf16[128,256]{1,0:T(8,128)(2,1)S(1)}, u32[]{:S(2)}, u32[]{:S(2)}) collective-permute-start(bf16[128,256]{1,0:T(8,128)(2,1)} %get-tuple-element.21), channel_id=1, source_target_pairs={{0,8},{8,16},{16,24},{24,32},{32,40},{40,48},{48,56},{56,64},{64,7... | collective-permute-start | bytes 196616 | tf_op jit(solution)/shard_map/ppermute | solution.py:37
  112.3 5.9 %collective-permute-start.1 = (bf16[128,256]{1,0:T(8,128)(2,1)}, bf16[128,256]{1,0:T(8,128)(2,1)S(1)}, u32[]{:S(2)}, u32[]{:S(2)}) collective-permute-start(bf16[128,256]{1,0:T(8,128)(2,1)} %get-tuple-element.22), channel_id=1, source_target_pairs={{8,0},{16,8},{24,16},{32,24},{40,32},{48,40},{56,48},{64,56},{72,6... | collective-permute-start | bytes 196616 | tf_op jit(solution)/shard_map/ppermute | solution.py:40
  118.3 1.1 fusion.73
  120.3 3.7 %bitcast_reduce_fusion = (f32[6,2,128]{2,1,0:T(2,128)S(1)}, f32[1024,6,128,2]{2,0,3,1:T(8,128)}) fusion(bf16[6,128,2,128]{3,1,2,0:T(8,128)(2,1)S(1)} %copy.27, bf16[1024,256]{1,0:T(8,128)(2,1)S(1)} %bitcast.144), kind=kOutput, calls=%fused_computation.1 | convolution fusion | flops 405797376 | bytes 6952960 | tf_op jit(solution)/shard_map/nqhgd,chd->nhgqc/dot_general | solution.py:193
  126.5 1.5 fusion.6
  128.1 3.8 %fusion.1 = f32[6,2,128]{2,1,0:T(2,128)S(1)} fusion(f32[1024,6,128,2]{2,0,3,1:T(8,128)} %get-tuple-element.41, f32[6,2,128]{2,1,0:T(2,128)S(1)} %maximum_maximum_fusion), kind=kLoop, calls=%fused_computation.5 | loop fusion | flops 4717056 | bytes 6303744 | tf_op jit(solution)/shard_map/reduce_sum | solution.py:210
  134.2 0.9 slice-done.1
  135.1 1.5 fusion.13
  137.0 1.0 convolution_convert_fusion
  138.0 41.2 %all_to_all.10 = bf16[8,96,2048]{2,1,0:T(8,128)(2,1)S(1)} all-to-all(bf16[8,96,2048]{2,1,0:T(8,128)(2,1)S(1)} %bitcast.139), channel_id=1, replica_groups=mesh['sp_0'=16,'sp_1'=4,'tp'=8] {'tp'}, dimensions={0} | all-to-all | bytes 6291456 | tf_op jit(solution)/shard_map/all_to_all | solution.py:68
  180.2 0.8 fusion.25
  (67 shorter events, 13.3 us)
Async XLA Ops:
  6.5 130.5 %copy-start = (bf16[256,2048]{1,0:T(8,128)(2,1)S(1)}, bf16[256,2048]{1,0:T(8,128)(2,1)}, u32[]{:S(2)}) copy-start(bf16[256,2048]{1,0:T(8,128)(2,1)} %param.25) | copy-start | bytes 3145732
  6.5 63.8 %copy-start.7 = (f32[2048]{0:T(1024)S(1)}, f32[2048]{0:T(1024)}, u32[]{:S(2)}) copy-start(f32[2048]{0:T(1024)} %param.17) | copy-start | bytes 24580
  6.5 63.8 %copy-start.4 = (bf16[16,2048]{1,0:T(8,128)(2,1)S(1)}, bf16[16,2048]{1,0:T(8,128)(2,1)}, u32[]{:S(2)}) copy-start(bf16[16,2048]{1,0:T(8,128)(2,1)} %param.16) | copy-start | bytes 196612
  6.5 63.8 %copy-start.3 = (bf16[2048,128]{1,0:T(8,128)(2,1)S(1)}, bf16[2048,128]{1,0:T(8,128)(2,1)}, u32[]{:S(2)}) copy-start(bf16[2048,128]{1,0:T(8,128)(2,1)} %param.22) | copy-start | bytes 1572868
  6.5 94.6 %all-gather.2.cloned.1.call-start = ((), (), s32[]{:S(2)}) async-start(), calls=%async_computation.2 | async-start | bytes 3538944 | tf_op jit(solution)/shard_map/all_gather | solution.py:133
  71.5 48.8 %all-to-all-start = ((bf16[64,16,256]{2,1,0:T(8,128)(2,1)}), bf16[64,16,256]{2,1,0:T(8,128)(2,1)S(1)}, u32[]{:S(2)}, u32[]{:S(2)}) async-start(bf16[64,16,256]{2,1,0:T(8,128)(2,1)} %broadcast_in_dim.12), calls=%async_computation | async-start | bytes 1048576 | tf_op jit(solution)/shard_map/all_to_all | solution.py:47
  86.2 18.9 %copy-start.5 = (bf16[2048,128]{1,0:T(8,128)(2,1)S(1)}, bf16[2048,128]{1,0:T(8,128)(2,1)}, u32[]{:S(2)}) copy-start(bf16[2048,128]{1,0:T(8,128)(2,1)} %param.23) | copy-start | bytes 1572868
  105.2 13.1 %copy-start.2 = (bf16[768,2048]{1,0:T(8,128)(2,1)S(1)}, bf16[768,2048]{1,0:T(8,128)(2,1)}, u32[]{:S(2)}) copy-start(bf16[768,2048]{1,0:T(8,128)(2,1)} %all-gather.2.cloned.1.call-done) | copy-start | bytes 9437188
  105.2 13.1 %copy-start.9 = (bf16[2048,256]{1,0:T(8,128)(2,1)S(1)}, bf16[2048,256]{1,0:T(8,128)(2,1)}, u32[]{:S(2)}) copy-start(bf16[2048,256]{1,0:T(8,128)(2,1)} %param.21) | copy-start | bytes 3145732
  108.9 16.4 %collective-permute-start = (bf16[128,256]{1,0:T(8,128)(2,1)}, bf16[128,256]{1,0:T(8,128)(2,1)S(1)}, u32[]{:S(2)}, u32[]{:S(2)}) collective-permute-start(bf16[128,256]{1,0:T(8,128)(2,1)} %get-tuple-element.21), channel_id=1, source_target_pairs={{0,8},{8,16},{16,24},{24,32},{32,40},{40,48},{48,56},{56,64},{64,7... | collective-permute-start | bytes 196616 | tf_op jit(solution)/shard_map/ppermute | solution.py:37
  112.3 13.0 %collective-permute-start.1 = (bf16[128,256]{1,0:T(8,128)(2,1)}, bf16[128,256]{1,0:T(8,128)(2,1)S(1)}, u32[]{:S(2)}, u32[]{:S(2)}) collective-permute-start(bf16[128,256]{1,0:T(8,128)(2,1)} %get-tuple-element.22), channel_id=1, source_target_pairs={{8,0},{16,8},{24,16},{32,24},{40,32},{48,40},{56,48},{64,56},{72,6... | collective-permute-start | bytes 196616 | tf_op jit(solution)/shard_map/ppermute | solution.py:40
  126.5 1.5 copy-start.8
  131.9 0.9 copy-start.6
  131.9 2.3 %slice-start = ((s8[6291456]{0:T(1024)(128)(4,1)}), s8[4194304]{0:T(1024)(128)(4,1)S(1)}, s32[]{:S(2)}) async-start(s8[6291456]{0:T(1024)(128)(4,1)} %bitcast.137), calls=%async_computation.3 | async-start | bytes 8388608
  132.8 2.2 %slice-start.1 = ((s8[6291456]{0:T(1024)(128)(4,1)}), s8[2097152]{0:T(1024)(128)(4,1)S(1)}, s32[]{:S(2)}) async-start(s8[6291456]{0:T(1024)(128)(4,1)} %bitcast.137), calls=%async_computation.4 | async-start | bytes 4194304
  179.2 1.0 copy-start.1
Sparse Core Ops, SparseCore 0:
  68.2 32.9 all-gather.1
where the time goes:
time: 189 us; the launch traced here: 188 us
  blocking collectives  96.1 us (51%)
  starting transfers between devices  21.6 us (11%)
  matrix products  19.7 us (10%)
  other arithmetic  15.8 us (8%)
  waiting for transfers between devices  15 us (8%)
  between operations  13.8 us (7%)
  local copies, waits for them, and re-layouts  5.96 us (3%)
    psum x2, blocking collectives, one_axis_at_a_time(): return functools.reduce(lax.psum, axes, x)  41.8 us
    all_to_all x1, blocking collectives, summed_on_arrival(): blocks = lax.all_to_all(in_blocks(x, dim, peers), axis, 0, 0, tiled=True)  41.2 us
    all_gather x1, waiting for transfers between devices, shards(): block_rows = lax.all_gather(hidden_state, 'tp', axis=0, tiled=True)  14.9 us
    all_gather x1, blocking collectives, side_by_side(): out, at, outs = (lax.all_gather(both, axis, axis=dim, tiled=True), 0, [])  13.1 us
    all_to_all x1, starting transfers between devices, sent_to_all(): lax.all_to_all(jnp.broadcast_to(x[None], (peers, *x.shape)), axis, 0, 0,...  12.3 us
    ppermute x1, starting transfers between devices, padded_2(): lax.ppermute(lax.slice_in_dim(block, 0, width, axis=dim), axis, backward)  5.93 us
    reduce_sum x1, other arithmetic, shards(): jnp.sum(ctx_exp, axis=-1, keepdims=True)  3.82 us
  transfers between devices with their start and end apart: 4, of which 1 were waited for; matrix products, arithmetic and copies ran while one was open for 11% of the time, Pallas kernels for 0%

commit v1 on v0

--- a/solution.py
+++ b/solution.py
@@ -113,6 +113,13 @@
     sink_logit_head,
     out_weight,
 ):
+
+    def _direct_stages_all(matrix):
+        top = lax.all_to_all(
+            jnp.concatenate(lax.axis_size("tp") * [matrix], axis=0), "tp", 0, 0, tiled=True
+        )
+        return top
+
     tp_count = lax.axis_size("tp")
     group_rows = latent.shape[0] * tp_count
     offset = lax.axis_index(SP) * group_rows
@@ -130,7 +137,7 @@
     hidden_state = modulated_norm(latent, norm_gain, shift_all[0], scale_all[0])
     query_width = query_weight.shape[1]
     pair_width = key_matrix.shape[1]
-    block_rows = lax.all_gather(hidden_state, "tp", axis=0, tiled=True)
+    block_rows = _direct_stages_all(hidden_state)
     row_count = block_rows.shape[0]
     position = offset + jnp.arange(row_count, dtype=jnp.int32)
     query_row_block = jnp.dot(block_rows, query_weight, preferred_element_type=jnp.float32)

time: 189 us -> 220 us (1.16)
  the two profiles are of different devices: /device:TPU:128 before, /device:TPU:1 now
where the time goes in v1:
time: 220 us; the launch traced here: 219 us
  blocking collectives  106 us (48%)
  waiting for transfers between devices  43.5 us (20%)
  other arithmetic  20.7 us (9%)
  matrix products  20.7 us (9%)
  starting transfers between devices  17.3 us (8%)
  local copies, waits for them, and re-layouts  10.2 us (5%)
    all_to_all x1, blocking collectives, summed_on_arrival(): blocks = lax.all_to_all(in_blocks(x, dim, peers), axis, 0, 0, tiled=True)  44 us
    psum x2, blocking collectives, one_axis_at_a_time(): return functools.reduce(lax.psum, axes, x)  39.6 us
    all_to_all x1, waiting for transfers between devices, _direct_stages_all(): lax.all_to_all(jnp.concatenate(lax.axis_size('tp') * [matrix], axis=0), '...  34.5 us
    all_gather x1, blocking collectives, side_by_side(): out, at, outs = (lax.all_gather(both, axis, axis=dim, tiled=True), 0, [])  22.7 us
    all_to_all x1, waiting for transfers between devices, sent_to_all(): lax.all_to_all(jnp.broadcast_to(x[None], (peers, *x.shape)), axis, 0, 0,...  9.01 us
    all_to_all x1, starting transfers between devices, sent_to_all(): lax.all_to_all(jnp.broadcast_to(x[None], (peers, *x.shape)), axis, 0, 0,...  7.64 us
    unnamed x30, local copies, waits for them, and re-layouts  5.73 us
    unnamed x8, other arithmetic  5.32 us
  transfers between devices with their start and end apart: 4, of which 2 were waited for; matrix products, arithmetic and copies ran while one was open for 11% of the time, Pallas kernels for 0%

profile of v1, /device:TPU:1, one launch (start us, length us, event | category | flops | bytes accessed | tf_op | source)
XLA Modules:
  0.0 219.0 jit_solution(5329146499534180506)
XLA Ops:
  0.0 1.3 fusion.20
  4.5 30.7 %all-reduce = (f32[1,256]{1,0:T(1,128)S(1)}, f32[2,256]{1,0:T(2,128)S(1)}, f32[2,256]{1,0:T(2,128)S(1)}) all-reduce(f32[1,256]{1,0:T(1,128)S(1)} %fusion.59, f32[2,256]{1,0:T(2,128)S(1)} %fusion.71, f32[2,256]{1,0:T(2,128)S(1)} %fusion.70), channel_id=1, replica_groups=mesh['sp_0'=16,'sp_1'=4,'tp'=8] {'sp_0'}, use_global_device_ids=true, to_apply=%region_4.5 | all-reduce | flops 1280 | bytes 10240 | tf_op jit(solution)/shard_map/psum | solution.py:20
  35.3 8.8 %all-reduce.1 = (f32[1,256]{1,0:T(1,128)S(1)}, f32[2,256]{1,0:T(2,128)S(1)}, f32[2,256]{1,0:T(2,128)S(1)}) all-reduce(f32[1,256]{1,0:T(1,128)S(1)} %get-tuple-element.5, f32[2,256]{1,0:T(2,128)S(1)} %get-tuple-element.6, f32[2,256]{1,0:T(2,128)S(1)} %get-tuple-element.7), channel_id=1, replica_groups=mesh['sp_0'=16,'sp_1'=4,'tp'=8] {'sp_1'}, use_global_device_ids=true, to_apply=%region_5.6 | all-reduce | flops 1280 | bytes 10240 | tf_op jit(solution)/shard_map/psum | solution.py:20
  44.1 22.7 %all_gather.3 = f32[5,2048]{1,0:T(8,128)S(1)} all-gather(f32[5,256]{1,0:T(8,128)S(1)} %pad_maximum_fusion.12), channel_id=1, replica_groups=mesh['sp_0'=16,'sp_1'=4,'tp'=8] {'tp'}, dimensions={1}, use_global_device_ids=true | all-gather | bytes 46080 | tf_op jit(solution)/shard_map/all_gather | solution.py:25
  68.1 1.2 constant_dynamic-update-slice_fusion.6
  72.4 1.7 copy-done.2
  74.1 4.6 %all-to-all-start = ((bf16[8,96,2048]{2,1,0:T(8,128)(2,1)}), bf16[8,96,2048]{2,1,0:T(8,128)(2,1)}, u32[]{:S(2)}, u32[]{:S(2)}) async-start(bf16[8,96,2048]{2,1,0:T(8,128)(2,1)} %bitcast.156), calls=%async_computation | async-start | bytes 6291456 | tf_op jit(solution)/shard_map/all_to_all | solution.py:118
  80.4 1.4 fusion.18
  81.8 34.5 %all-to-all-done = bf16[8,96,2048]{2,1,0:T(8,128)(2,1)} async-done(((bf16[8,96,2048]{2,1,0:T(8,128)(2,1)}), bf16[8,96,2048]{2,1,0:T(8,128)(2,1)}, u32[]{:S(2)}, u32[]{:S(2)}) %all-to-all-start) | async-done | bytes 3145760 | tf_op jit(solution)/shard_map/all_to_all | solution.py:118
  117.1 7.6 %all-to-all-start.1 = ((bf16[64,16,256]{2,1,0:T(8,128)(2,1)}), bf16[64,16,256]{2,1,0:T(8,128)(2,1)S(1)}, u32[]{:S(2)}, u32[]{:S(2)}) async-start(bf16[64,16,256]{2,1,0:T(8,128)(2,1)} %broadcast_in_dim.12), calls=%async_computation.1 | async-start | bytes 1048576 | tf_op jit(solution)/shard_map/all_to_all | solution.py:47
  124.8 1.4 fusion.39
  127.2 1.5 copy.32
  128.7 2.9 %fusion.72 = f32[768,2,2,2,32]{0,4,3,2,1:T(8,128)S(1)} fusion(bf16[768,2048,1,1,1]{1,0,4,3,2:T(8,128)(2,1)} %bitcast.30, bf16[2,2,2,32,2048]{4,3,2,1,0:T(8,128)(2,1)S(1)} %bitcast.162), kind=kOutput, calls=%fused_computation.135 | convolution fusion | flops 805306368 | bytes 4980736 | tf_op jit(solution)/shard_map/dot_general | solution.py:143
  132.6 3.2 %convolution_bitcast_fusion.1 = f32[768,1,2,2,32]{0,4,3,2,1:T(8,128)S(1)} fusion(bf16[768,2048,1,1]{1,0,3,2:T(8,128)(2,1)} %bitcast.11, bf16[2,2,32,2048]{3,2,1,0:T(8,128)(2,1)} %bitcast.181), kind=kOutput, calls=%fused_computation.19 | convolution fusion | flops 402653184 | bytes 4063232 | tf_op jit(solution)/shard_map/dot_general | solution.py:145
  136.7 3.0 %convolution_convert_fusion.1 = bf16[768,128]{1,0:T(8,128)(2,1)S(1)} fusion(bf16[768,2048]{1,0:T(8,128)(2,1)} %bitcast.9, bf16[2048,128]{1,0:T(8,128)(2,1)} %param.23), kind=kOutput, calls=%fused_computation.28 | convolution fusion | flops 402751488 | bytes 3866624 | tf_op jit(solution)/shard_map/dot_general | solution.py:147
  140.4 3.6 %collective-permute-start = (bf16[128,256]{1,0:T(8,128)(2,1)}, bf16[128,256]{1,0:T(8,128)(2,1)}, u32[]{:S(2)}, u32[]{:S(2)}) collective-permute-start(bf16[128,256]{1,0:T(8,128)(2,1)} %get-tuple-element.21), channel_id=1, source_target_pairs={{0,8},{8,16},{16,24},{24,32},{32,40},{40,48},{48,56},{56,64},{64,7... | collective-permute-start | bytes 196616 | tf_op jit(solution)/shard_map/ppermute | solution.py:37
  143.9 1.5 collective-permute-start.1
  145.4 9.0 %all-to-all-done.1 = bf16[64,16,256]{2,1,0:T(8,128)(2,1)S(1)} async-done(((bf16[64,16,256]{2,1,0:T(8,128)(2,1)}), bf16[64,16,256]{2,1,0:T(8,128)(2,1)S(1)}, u32[]{:S(2)}, u32[]{:S(2)}) %all-to-all-start.1) | async-done | bytes 524320 | tf_op jit(solution)/shard_map/all_to_all | solution.py:47
  154.4 3.6 %bitcast_reduce_fusion = (f32[6,2,128]{2,1,0:T(2,128)S(1)}, f32[1024,6,128,2]{2,0,3,1:T(8,128)}) fusion(bf16[6,128,2,128]{3,1,2,0:T(8,128)(2,1)S(1)} %copy.33, bf16[1024,256]{1,0:T(8,128)(2,1)S(1)} %bitcast.160), kind=kOutput, calls=%fused_computation.1 | convolution fusion | flops 405797376 | bytes 6952960 | tf_op jit(solution)/shard_map/nqhgd,chd->nhgqc/dot_general | solution.py:200
  160.0 1.6 pad_maximum_fusion.6
  162.0 1.6 fusion.6
  163.7 3.9 %fusion.1 = f32[6,2,128]{2,1,0:T(2,128)S(1)} fusion(f32[1024,6,128,2]{2,0,3,1:T(8,128)} %get-tuple-element.41, f32[6,2,128]{2,1,0:T(2,128)S(1)} %maximum_maximum_fusion), kind=kLoop, calls=%fused_computation.5 | loop fusion | flops 4717056 | bytes 6303744 | tf_op jit(solution)/shard_map/reduce_sum | solution.py:217
  170.6 1.5 fusion.13
  173.5 44.0 %all_to_all.22 = bf16[8,96,2048]{2,1,0:T(8,128)(2,1)S(1)} all-to-all(bf16[8,96,2048]{2,1,0:T(8,128)(2,1)S(1)} %bitcast.155), channel_id=1, replica_groups=mesh['sp_0'=16,'sp_1'=4,'tp'=8] {'tp'}, dimensions={0} | all-to-all | bytes 6291456 | tf_op jit(solution)/shard_map/all_to_all | solution.py:68
  (79 shorter events, 21.7 us)
Async XLA Ops:
  0.0 172.5 %copy-start = (bf16[256,2048]{1,0:T(8,128)(2,1)S(1)}, bf16[256,2048]{1,0:T(8,128)(2,1)}, u32[]{:S(2)}) copy-start(bf16[256,2048]{1,0:T(8,128)(2,1)} %param.25) | copy-start | bytes 3145732
  0.0 70.6 %copy-start.1 = (bf16[96,2048]{1,0:T(8,128)(2,1)S(1)}, bf16[96,2048]{1,0:T(8,128)(2,1)}, u32[]{:S(2)}) copy-start(bf16[96,2048]{1,0:T(8,128)(2,1)} %param.13) | copy-start | bytes 1179652
  0.0 71.5 %copy-start.4 = (f32[2048]{0:T(1024)S(1)}, f32[2048]{0:T(1024)}, u32[]{:S(2)}) copy-start(f32[2048]{0:T(1024)} %param.17) | copy-start | bytes 24580
  72.4 1.7 copy-start.2
  74.1 4.7 %copy-start.6 = (bf16[16,2048]{1,0:T(8,128)(2,1)S(1)}, bf16[16,2048]{1,0:T(8,128)(2,1)}, u32[]{:S(2)}) copy-start(bf16[16,2048]{1,0:T(8,128)(2,1)} %param.16) | copy-start | bytes 196612
  74.1 4.8 %copy-start.7 = (bf16[2048,128]{1,0:T(8,128)(2,1)S(1)}, bf16[2048,128]{1,0:T(8,128)(2,1)}, u32[]{:S(2)}) copy-start(bf16[2048,128]{1,0:T(8,128)(2,1)} %param.23) | copy-start | bytes 1572868
  74.1 5.1 %copy-start.3 = (bf16[2048,128]{1,0:T(8,128)(2,1)S(1)}, bf16[2048,128]{1,0:T(8,128)(2,1)}, u32[]{:S(2)}) copy-start(bf16[2048,128]{1,0:T(8,128)(2,1)} %param.22) | copy-start | bytes 1572868
  74.1 42.2 %all-to-all-start = ((bf16[8,96,2048]{2,1,0:T(8,128)(2,1)}), bf16[8,96,2048]{2,1,0:T(8,128)(2,1)}, u32[]{:S(2)}, u32[]{:S(2)}) async-start(bf16[8,96,2048]{2,1,0:T(8,128)(2,1)} %bitcast.156), calls=%async_computation | async-start | bytes 6291456 | tf_op jit(solution)/shard_map/all_to_all | solution.py:118
  117.1 37.3 %all-to-all-start.1 = ((bf16[64,16,256]{2,1,0:T(8,128)(2,1)}), bf16[64,16,256]{2,1,0:T(8,128)(2,1)S(1)}, u32[]{:S(2)}, u32[]{:S(2)}) async-start(bf16[64,16,256]{2,1,0:T(8,128)(2,1)} %broadcast_in_dim.12), calls=%async_computation.1 | async-start | bytes 1048576 | tf_op jit(solution)/shard_map/all_to_all | solution.py:47
  128.6 3.0 %copy-start.5 = (f32[768,2,32]{0,2,1:T(8,128)S(1)}, f32[768,2,32]{0,2,1:T(8,128)}, u32[]{:S(2)}) copy-start(f32[768,2,32]{0,2,1:T(8,128)} %get-tuple-element.24) | copy-start | bytes 589828
  132.6 3.2 %copy-start.8 = (f32[768,1,1,1,32]{0,4,3,2,1:T(8,128)S(1)}, f32[768,1,1,1,32]{0,4,3,2,1:T(8,128)}, u32[]{:S(2)}) copy-start(f32[768,1,1,1,32]{0,4,3,2,1:T(8,128)} %get-tuple-element.30) | copy-start | bytes 294916
  132.6 3.2 %copy-start.9 = (f32[768,1,1,1,32]{0,4,3,2,1:T(8,128)S(1)}, f32[768,1,1,1,32]{0,4,3,2,1:T(8,128)}, u32[]{:S(2)}) copy-start(f32[768,1,1,1,32]{0,4,3,2,1:T(8,128)} %get-tuple-element.37) | copy-start | bytes 294916
  140.4 19.6 %collective-permute-start = (bf16[128,256]{1,0:T(8,128)(2,1)}, bf16[128,256]{1,0:T(8,128)(2,1)}, u32[]{:S(2)}, u32[]{:S(2)}) collective-permute-start(bf16[128,256]{1,0:T(8,128)(2,1)} %get-tuple-element.21), channel_id=1, source_target_pairs={{0,8},{8,16},{16,24},{24,32},{32,40},{40,48},{48,56},{56,64},{64,7... | collective-permute-start | bytes 196616 | tf_op jit(solution)/shard_map/ppermute | solution.py:37
  143.9 16.0 %collective-permute-start.1 = (bf16[128,256]{1,0:T(8,128)(2,1)}, bf16[128,256]{1,0:T(8,128)(2,1)}, u32[]{:S(2)}, u32[]{:S(2)}) collective-permute-start(bf16[128,256]{1,0:T(8,128)(2,1)} %get-tuple-element.22), channel_id=1, source_target_pairs={{8,0},{16,8},{24,16},{32,24},{40,32},{48,40},{56,48},{64,56},{72,6... | collective-permute-start | bytes 196616 | tf_op jit(solution)/shard_map/ppermute | solution.py:40
  160.0 3.6 %copy-start.11 = (f32[2]{0:T(128)S(1)}, f32[2]{0:T(128)}, u32[]{:S(2)}) copy-start(f32[2]{0:T(128)} %param.24) | copy-start | bytes 28
  163.7 4.5 %copy-start.10 = (bf16[6,128,1,128]{1,3,0,2:T(8,128)(2,1)S(1)}, bf16[6,128,1,128]{1,3,0,2:T(8,128)(2,1)}, u32[]{:S(2)}) copy-start(bf16[6,128,1,128]{1,3,0,2:T(8,128)(2,1)} %copy.29) | copy-start | bytes 589828
  167.6 2.2 slice-start
  168.2 2.4 %slice-start.1 = ((s8[6291456]{0:T(1024)(128)(4,1)}), s8[2097152]{0:T(1024)(128)(4,1)S(1)}, s32[]{:S(2)}) async-start(s8[6291456]{0:T(1024)(128)(4,1)} %bitcast.153), calls=%async_computation.4 | async-start | bytes 4194304
